TPU v7x, 256 devices: a whole 4x4x8 slice. The times are simulated.
256 devices in a mesh: ep: 64 (over z, y, core), tp: 4 (over x).
Axes of the slice: x: 4, y: 4, z: 8, core: 2. Of those that a mesh axis runs over, the one named last changes fastest.
Arguments:
- conv_value: bfloat16 [24576, 2048], P('ep', 'tp'), may hold values from -36 to 36
- conv_gate: bfloat16 [24576, 2048], P('ep', 'tp'), may hold values from -8 to 8
- conv_taps: bfloat16 [31, 2048], P(None, 'tp'), may hold values from -1 to 1
- conv_gain: float32 [2048], P('tp'), may hold values from 0.1 to 1.9
- conv_proj: bfloat16 [2048, 2048], P('tp'), may hold values from -0.125 to 0.125
- moe_tokens: bfloat16 [24576, 2048], P('ep'), may hold values from -6 to 6
- moe_gain: float32 [2048], replicated, may hold values from 0.1 to 1.9
- routes: int32 [24576, 2], P('ep'), may hold values from 0 to 63, all different within a row; in each aligned block of 384 rows (0 to 383, 384 to 767, ...) at most 18 rows name the same one
- route_weights: float32 [24576, 2], P('ep'), may hold values from 0.3 to 3
- expert_gate: bfloat16 [64, 2048, 1024], P('ep', None, 'tp'), may hold values from -0.125 to 0.125
- expert_up: bfloat16 [64, 2048, 1024], P('ep', None, 'tp'), may hold values from -0.125 to 0.125
- expert_down: bfloat16 [64, 1024, 2048], P('ep', 'tp'), may hold values from -0.1875 to 0.1875
- shared_gate: bfloat16 [2048, 256], replicated, may hold values from -0.125 to 0.125
- shared_up: bfloat16 [2048, 256], replicated, may hold values from -0.125 to 0.125
- shared_down: bfloat16 [256, 2048], P(None, 'tp'), may hold values from -0.375 to 0.375
Outputs:
- conv_result: bfloat16 [24576, 2048], P('ep', 'tp')
- moe_result: bfloat16 [24576, 2048], P('ep', 'tp')
Inputs may be any that keep to these rules, and one draw needn't show every extreme that they name: `routes`: each row names 2 different experts. Among the 384 rows of one index of ep (aligned blocks in order) no expert is named more than 18 times, and in some blocks one expert is named exactly 18 times.
All inputs are finite; a program needn't handle non-finite values.
Results may differ from a plain program's by a relative error of at most 0.01.
Values may be sent and summed in bfloat16 or wider, within the bound.
A program may use at most 64 MiB of HBM per device.

v0:
```python
import jax
import jax.numpy as jnp
from jax import lax
from jax.sharding import PartitionSpec as P

epsilon = 1e-05


def passed_along(value, axis, by):
    devices = lax.axis_size(axis)
    pairs = [(i, i + by) for i in range(devices) if 0 <= i + by < devices]
    return lax.ppermute(value, axis, pairs)


def total_of_pieces(value, axis):
    parts = lax.all_gather(value, axis)
    return parts.sum(axis=0)


def shared_hidden_rows(rows, shared_gate, shared_up):
    return (
        jax.nn.silu(jnp.dot(rows, shared_gate, preferred_element_type=jnp.float32))
        * jnp.dot(rows, shared_up, preferred_element_type=jnp.float32)
    ).astype(jnp.bfloat16)


def local(
    conv_value,
    conv_gate,
    conv_taps,
    conv_gain,
    conv_proj,
    moe_tokens,
    moe_gain,
    routes,
    route_weights,
    expert_gate,
    expert_up,
    expert_down,
    shared_gate,
    shared_up,
    shared_down,
):
    model_width = moe_tokens.shape[1]
    tok_rows = conv_value.shape[0]
    kernel = conv_taps.shape[0]
    gated_rows = (
        conv_value.astype(jnp.float32) * jax.nn.sigmoid(conv_gate.astype(jnp.float32))
    ).astype(jnp.bfloat16)
    previous = passed_along(gated_rows[tok_rows - (kernel - 1) :], "ep", 1)
    padded = jnp.concatenate([previous, gated_rows], axis=0).astype(jnp.float32)
    tap_weights = conv_taps.astype(jnp.float32)
    convolved = jnp.zeros(gated_rows.shape, jnp.float32)
    for offset in range(kernel):
        convolved = convolved + tap_weights[offset][None, :] * padded[offset : offset + tok_rows]
    total_sum, square_sum = (
        total_of_pieces(jnp.sum(convolved, axis=1), "tp"),
        total_of_pieces(jnp.sum(convolved * convolved, axis=1), "tp"),
    )
    average = total_sum / model_width
    variance = square_sum / model_width - average * average
    scaled = (
        (convolved - average[:, None]) * lax.rsqrt(variance + epsilon)[:, None] * conv_gain[None, :]
    )
    activated = jax.nn.silu(scaled).astype(jnp.bfloat16)
    conv_partial = jnp.dot(activated, conv_proj, preferred_element_type=jnp.float32)
    tokens = moe_tokens.astype(jnp.float32)
    token_mean = jnp.mean(tokens, axis=1, keepdims=True)
    centered = tokens - token_mean
    token_var = jnp.mean(centered * centered, axis=1, keepdims=True)
    normalized = (centered * lax.rsqrt(token_var + epsilon) * moe_gain[None, :]).astype(
        jnp.bfloat16
    )
    shared_hidden = shared_hidden_rows(normalized, shared_gate, shared_up)
    shared_part = jnp.dot(shared_hidden, shared_down, preferred_element_type=jnp.float32)
    experts = lax.axis_size("ep")
    top_count = routes.shape[1]
    capacity = 3 * tok_rows * top_count // (2 * experts)
    entries = tok_rows * top_count
    flat_routes = routes.reshape(-1)
    one_hot = (flat_routes[:, None] == jnp.arange(experts, dtype=jnp.int32)[None, :]).astype(
        jnp.int32
    )
    before = jnp.cumsum(one_hot, axis=0) - one_hot
    slot_rank = jnp.sum(before * one_hot, axis=1)
    slot_index = flat_routes * capacity + slot_rank
    source_row = (
        jnp.full((experts * capacity,), -1, jnp.int32)
        .at[slot_index]
        .set(jnp.arange(entries, dtype=jnp.int32))
    )
    filled = source_row >= 0
    token_index = jnp.where(filled, source_row // top_count, 0)
    outgoing = jnp.where(filled[:, None], normalized[token_index], jnp.zeros((), jnp.bfloat16))
    outgoing = outgoing.reshape(experts, capacity, model_width)
    quarter = model_width // lax.axis_size("tp")
    first_column = lax.axis_index("tp") * quarter
    column_block = lax.dynamic_slice_in_dim(outgoing, first_column, quarter, 2)
    arrived = lax.all_to_all(column_block, "ep", split_axis=0, concat_axis=0, tiled=True)
    arrived = lax.all_gather(arrived, "tp", axis=2, tiled=True)
    expert_input = arrived.reshape(experts * capacity, model_width)
    hidden = (
        jax.nn.silu(jnp.dot(expert_input, expert_gate[0], preferred_element_type=jnp.float32))
        * jnp.dot(expert_input, expert_up[0], preferred_element_type=jnp.float32)
    ).astype(jnp.bfloat16)
    expert_partial = jnp.dot(hidden, expert_down[0], preferred_element_type=jnp.float32)
    conv_sum, expert_sum = (
        lax.psum_scatter(
            conv_partial.astype(jnp.bfloat16), "tp", scatter_dimension=1, tiled=True
        ).astype(jnp.float32),
        lax.psum_scatter(
            expert_partial.astype(jnp.bfloat16), "tp", scatter_dimension=1, tiled=True
        ).astype(jnp.float32),
    )
    conv_result = conv_sum.astype(jnp.bfloat16)
    expert_rows = expert_sum.astype(jnp.bfloat16).reshape(experts, capacity, expert_sum.shape[1])
    returned = lax.all_to_all(expert_rows, "ep", split_axis=0, concat_axis=0, tiled=True)
    picked = returned.reshape(experts * capacity, returned.shape[2])[slot_index]
    picked = picked.astype(jnp.float32).reshape(tok_rows, top_count, returned.shape[2])
    moe_result = (shared_part + jnp.sum(route_weights[:, :, None] * picked, axis=1)).astype(
        jnp.bfloat16
    )
    return (conv_result, moe_result)


def solution(mesh):
    placed = (
        P("ep", "tp"),
        P("ep", "tp"),
        P(None, "tp"),
        P("tp"),
        P("tp", None),
        P("ep", None),
        P(),
        P("ep", None),
        P("ep", None),
        P("ep", None, "tp"),
        P("ep", None, "tp"),
        P("ep", "tp", None),
        P(),
        P(),
        P(None, "tp"),
    )
    return jax.shard_map(
        local, mesh=mesh, in_specs=placed, out_specs=(P("ep", "tp"), P("ep", "tp")), check_vma=False
    )
```

profile of v0, /device:TPU:1, one launch (start us, length us, event | category | flops | bytes accessed | tf_op | source)
XLA Modules:
  0.0 311.6 jit_solution(3662823600982574159)
XLA Ops:
  7.2 0.0 copy-start
  7.2 0.0 all-gather.6.cloned.1.call-start
  7.2 1.0 copy.25
  8.2 0.1 eq.29
  8.3 0.1 eq.25
  8.5 0.7 broadcast_multiply_fusion
  9.2 1.8 reduce-window.6
  11.0 0.3 slice_reduce_fusion
  11.3 0.1 copy.24
  11.4 0.2 mul.517
  11.6 0.1 fusion.60
  11.8 3.4 %scatter_custom_fusion = s32[1152]{0:T(1024)S(1)} fusion(s32[768]{0:T(1024)S(1)} %fusion.68, s32[768]{0:T(1024)S(1)} %iota.11, s32[]{:T(128)} %constant.26.clone.1), kind=kCustom, calls=%fused_computation.127 | custom fusion | bytes 4612 | tf_op jit(solution)/shard_map/scatter | solution.py:90
  15.2 0.0 copy-start.1
  15.2 0.0 copy-start.5
  15.2 1.8 convert_reduce_fusion
  17.1 0.0 copy-done.1
  17.1 0.6 fusion.2
  17.6 0.0 copy-done.5
  17.6 1.7 fusion.4
  19.3 12.3 %gather_fusion = bf16[1152,2048]{1,0:T(8,128)(2,1)} fusion(bf16[384,2048]{1,0:T(8,128)(2,1)} %fusion.4, s32[2048]{0:T(1024)S(1)} %pad_clamp_fusion), kind=kCustom, calls=%fused_computation | custom fusion | bytes 9441792 | tf_op jit(solution)/shard_map/gather | solution.py:94
  31.6 7.6 %gather.9 = bf16[64,18,2048]{2,1,0:T(8,128)(2,1)} reshape(bf16[1152,2048]{1,0:T(8,128)(2,1)} %gather_fusion) | data formatting | bytes 9437184 | tf_op jit(solution)/shard_map/gather | solution.py:94
  39.2 0.1 broadcast_in_dim.21
  39.3 1.8 dynamic-slice_select_fusion
  41.2 52.1 %all_to_all.10 = bf16[64,18,512]{2,1,0:T(8,128)(2,1)} all-to-all(bf16[64,18,512]{2,1,0:T(8,128)(2,1)S(1)} %dynamic-slice_select_fusion), channel_id=1, replica_groups=mesh['ep'=64,'tp'=4] {'ep'}, dimensions={0} | all-to-all | bytes 2359296 | tf_op jit(solution)/shard_map/all_to_all | solution.py:99
  93.3 0.0 all-gather.6.cloned.1.call-update
  93.3 0.2 reduce-scatter.5.cloned.1.call-start
  93.5 64.9 %all-gather.6.cloned.1.call-done = bf16[64,18,2048]{2,1,0:T(8,128)(2,1)} async-done(((bf16[64,18,512]{2,1,0:T(8,128)(2,1)}), bf16[64,18,2048]{2,1,0:T(8,128)(2,1)}) %all-gather.6.cloned.1.call-update) | async-done | bytes 4718608 | tf_op jit(solution)/shard_map/all_gather | solution.py:100
  158.5 7.8 %reshape.99 = bf16[1152,2048]{1,0:T(8,128)(2,1)} reshape(bf16[64,18,2048]{2,1,0:T(8,128)(2,1)} %all-gather.6.cloned.1.call-done) | data formatting | bytes 9437184 | tf_op jit(solution)/shard_map/reshape | solution.py:101
  166.2 5.1 %fusion.16 = f32[1152,256]{1,0:T(8,128)} fusion(bf16[1152,2048]{1,0:T(8,128)(2,1)} %reshape.99, bf16[1,2048,256]{2,1,0:T(8,128)(2,1)} %param.24), kind=kOutput, calls=%fused_computation.27 | convolution fusion | flops 1207959552 | bytes 6946816 | tf_op jit(solution)/shard_map/dot_general | solution.py:103
  171.3 10.3 %convolution_convert_fusion = bf16[1152,2048]{1,0:T(8,128)(2,1)} fusion(bf16[1152,2048]{1,0:T(8,128)(2,1)} %reshape.99, f32[1152,256]{1,0:T(8,128)} %fusion.16, bf16[1,256,2048]{2,1,0:T(8,128)(2,1)} %param.26, bf16[1,2048,256]{2,1,0:T(8,128)(2,1)} %param.25), kind=kOutput, calls=%fused_computation.3 | convolution fusion | flops 2420047872 | bytes 12713984 | tf_op jit(solution)/shard_map/dot_general | solution.py:106
  181.6 0.0 copy-start.2
  181.6 0.0 copy-start.3
  181.6 0.0 copy-start.4
  181.6 0.0 reduce-scatter.5.cloned.1.call-update
  181.6 0.0 reduce-scatter.3.cloned.1.call-start
  181.7 0.9 copy-done.2
  182.6 0.1 copy-done.3
  182.7 0.2 multiply_convert_fusion.1
  182.9 3.8 %collective-permute-start = (bf16[30,512]{1,0:T(8,128)(2,1)S(1)}, bf16[30,512]{1,0:T(8,128)(2,1)S(1)}, u32[]{:S(2)}, u32[]{:S(2)}) collective-permute-start(bf16[30,512]{1,0:T(8,128)(2,1)S(1)} %slice.265), channel_id=1, source_target_pairs={{0,4},{4,8},{8,12},{12,16},{16,20},{20,24},{24,28},{28,32},{32,36}... | collective-permute-start | bytes 92168 | tf_op jit(solution)/shard_map/ppermute | solution.py:12
  186.8 0.0 copy-done.4
  186.9 0.9 collective-permute-done
  187.8 0.1 maximum_convert_fusion
  187.9 0.0 copy-start.8
  187.9 3.8 %fusion.72 = (f32[384]{0:T(512)S(1)}, f32[384]{0:T(512)S(1)}, f32[384,512]{1,0:T(8,128)S(1)}) fusion(f32[414,512]{1,0:T(8,128)S(1)} %maximum_convert_fusion, f32[512]{0:T(512)S(1)} %bitcast.100, f32[512]{0:T(512)S(1)} %bitcast.99, f32[512]{0:T(512)S(1)} %bitcast.98, f32[512]{0:T(512)S(1)} %bitcast.97, f32[512]{0:T(512)S(1)} %bitcast.96, ...), kind=kLoop, calls=%fused_computation.138 | loop fusion | flops 12582144 | bytes 25232384 | tf_op jit(solution)/shard_map/reduce_sum | solution.py:57
  191.8 9.1 %all-gather.2 = f32[4,1,384]{2,1,0:T(1,128)S(1)} all-gather(f32[1,1,384]{2,1,0:T(1,128)S(1)} %reshape.130), channel_id=2, replica_groups=mesh['ep'=64,'tp'=4] {'tp'}, dimensions={0}, use_global_device_ids=true | all-gather | bytes 7680 | tf_op jit(solution)/shard_map/all_gather | solution.py:16
  200.9 9.6 %all-gather.3 = f32[4,1,384]{2,1,0:T(1,128)S(1)} all-gather(f32[1,1,384]{2,1,0:T(1,128)S(1)} %reshape.132), channel_id=3, replica_groups=mesh['ep'=64,'tp'=4] {'tp'}, dimensions={0}, use_global_device_ids=true | all-gather | bytes 7680 | tf_op jit(solution)/shard_map/all_gather | solution.py:16
  210.5 0.0 copy-done
  210.5 0.0 copy-done.8
  210.5 2.3 convolution_convert_fusion.1
  212.8 0.0 reduce-scatter.3.cloned.1.call-update
  212.9 23.5 %reduce-scatter.5.cloned.1.call-done = bf16[1152,512]{1,0:T(8,128)(2,1)} async-done(((bf16[1152,2048]{1,0:T(8,128)(2,1)}), bf16[1152,512]{1,0:T(8,128)(2,1)}) %reduce-scatter.5.cloned.1.call-update) | async-done | bytes 1179664 | tf_op jit(solution)/shard_map/reduce_scatter | solution.py:111
  236.4 3.0 reshape.100
  239.4 0.0 copy-start.6
  239.4 11.1 %all-to-all-start.1 = ((bf16[64,18,512]{2,1,0:T(8,128)(2,1)}), bf16[64,18,512]{2,1,0:T(8,128)(2,1)}, u32[]{:S(2)}, u32[]{:S(2)}) async-start(bf16[64,18,512]{2,1,0:T(8,128)(2,1)} %reshape.100), calls=%async_computation.3 | async-start | bytes 3145728 | tf_op jit(solution)/shard_map/all_to_all | solution.py:117
  250.5 0.0 copy-done.6
  250.5 0.1 copy.23
  250.7 3.1 fusion.76
  253.7 35.8 %all-to-all-done.1 = bf16[64,18,512]{2,1,0:T(8,128)(2,1)} async-done(((bf16[64,18,512]{2,1,0:T(8,128)(2,1)}), bf16[64,18,512]{2,1,0:T(8,128)(2,1)}, u32[]{:S(2)}, u32[]{:S(2)}) %all-to-all-start.1) | async-done | bytes 1179680 | tf_op jit(solution)/shard_map/all_to_all | solution.py:117
  289.5 2.3 reshape.101
  291.8 3.3 %gather_fusion.1 = bf16[768,512]{1,0:T(8,128)(2,1)} fusion(bf16[1152,512]{1,0:T(8,128)(2,1)S(1)} %reshape.101, s32[1024]{0:T(1024)S(1)} %pad_clamp_fusion.1), kind=kCustom, calls=%fused_computation.1 | custom fusion | bytes 1575936 | tf_op jit(solution)/shard_map/gather | solution.py:118
  295.1 3.0 reshape.102
  298.1 3.6 %multiply_reduce_fusion = f32[384,512]{1,0:T(8,128)S(1)} fusion(f32[384,2,512]{2,1,0:T(2,128)} %reshape.102, f32[384,2]{1,0:T(8,128)S(1)} %copy.23), kind=kLoop, calls=%fused_computation.15 | loop fusion | flops 589824 | bytes 2362368 | tf_op jit(solution)/shard_map/reduce_sum | solution.py:120
  301.7 0.0 copy-done.7
  301.7 3.4 %fusion.6 = bf16[384,512]{1,0:T(8,128)(2,1)} fusion(f32[384,512]{1,0:T(8,128)S(1)} %multiply_reduce_fusion, bf16[256,512]{1,0:T(8,128)(2,1)S(1)} %copy-done.7, bf16[384,2048]{1,0:T(8,128)(2,1)} %fusion.4, bf16[2048,256]{1,0:T(8,128)(2,1)} %param.28, f32[384,256]{1,0:T(8,128)} %fusion.76), kind=kOutput, calls=%fused_computation.17 | convolution fusion | flops 504299520 | bytes 4456448 | tf_op jit(solution)/shard_map/dot_general | solution.py:75
  (20 shorter events, 0.2 us)
Async XLA Ops:
  7.2 203.3 %copy-start = (bf16[512,2048]{1,0:T(8,128)(2,1)S(1)}, bf16[512,2048]{1,0:T(8,128)(2,1)}, u32[]{:S(2)}) copy-start(bf16[512,2048]{1,0:T(8,128)(2,1)} %param.19) | copy-start | bytes 6291460
  7.2 151.3 %all-gather.6.cloned.1.call-start = ((), (), s32[]{:S(2)}) async-start(), calls=%async_computation.5 | async-start | bytes 7864320 | tf_op jit(solution)/shard_map/all_gather | solution.py:100
  15.2 1.9 copy-start.1
  15.2 2.4 copy-start.5
  93.3 143.1 %reduce-scatter.5.cloned.1.call-start = ((), (), s32[]{:S(2)}) async-start(), calls=%async_computation.6 | async-start | bytes 5898240 | tf_op jit(solution)/shard_map/reduce_scatter | solution.py:111
  181.6 1.0 copy-start.2
  181.6 1.1 copy-start.3
  181.6 5.2 %copy-start.4 = (bf16[31,512]{1,0:T(8,128)(2,1)S(1)}, bf16[31,512]{1,0:T(8,128)(2,1)}, u32[]{:S(2)}) copy-start(bf16[31,512]{1,0:T(8,128)(2,1)} %param.17) | copy-start | bytes 95236
  181.6 123.5 %reduce-scatter.3.cloned.1.call-start = ((), (), s32[]{:S(2)}) async-start(), calls=%async_computation.4 | async-start | bytes 1966080 | tf_op jit(solution)/shard_map/reduce_scatter | solution.py:108
  182.9 4.9 %collective-permute-start = (bf16[30,512]{1,0:T(8,128)(2,1)S(1)}, bf16[30,512]{1,0:T(8,128)(2,1)S(1)}, u32[]{:S(2)}, u32[]{:S(2)}) collective-permute-start(bf16[30,512]{1,0:T(8,128)(2,1)S(1)} %slice.265), channel_id=1, source_target_pairs={{0,4},{4,8},{8,12},{12,16},{16,20},{20,24},{24,28},{28,32},{32,36}... | collective-permute-start | bytes 92168 | tf_op jit(solution)/shard_map/ppermute | solution.py:12
  187.9 22.6 %copy-start.8 = (f32[512]{0:T(512)S(1)}, f32[512]{0:T(512)}, u32[]{:S(2)}) copy-start(f32[512]{0:T(512)} %param.18) | copy-start | bytes 6148
  239.4 11.1 %copy-start.6 = (f32[384,2]{0,1:T(2,128)S(1)}, f32[384,2]{0,1:T(2,128)}, u32[]{:S(2)}) copy-start(f32[384,2]{0,1:T(2,128)} %param.23) | copy-start | bytes 9220
  239.4 50.1 %all-to-all-start.1 = ((bf16[64,18,512]{2,1,0:T(8,128)(2,1)}), bf16[64,18,512]{2,1,0:T(8,128)(2,1)}, u32[]{:S(2)}, u32[]{:S(2)}) async-start(bf16[64,18,512]{2,1,0:T(8,128)(2,1)} %reshape.100), calls=%async_computation.3 | async-start | bytes 3145728 | tf_op jit(solution)/shard_map/all_to_all | solution.py:117
  298.1 3.6 %copy-start.7 = (bf16[256,512]{1,0:T(8,128)(2,1)S(1)}, bf16[256,512]{1,0:T(8,128)(2,1)}, u32[]{:S(2)}) copy-start(bf16[256,512]{1,0:T(8,128)(2,1)} %param.29) | copy-start | bytes 786436
Sparse Core Ops, SparseCore 0:
  93.4 65.0 all-gather.5
  181.7 54.6 reduce-scatter.4
  239.5 27.0 reduce-scatter.2
where the time goes:
time: 313 us; the launch traced here: 312 us
  waiting for transfers between devices  125 us (40%)
  blocking collectives  70.7 us (23%)
  local copies, waits for them, and re-layouts  45.9 us (15%)
  matrix products  24.2 us (8%)
  other arithmetic  16.4 us (5%)
  starting transfers between devices  15.2 us (5%)
  between operations  14 us (4%)
    all_gather x1, waiting for transfers between devices, local(): arrived = lax.all_gather(arrived, 'tp', axis=2, tiled=True)  64.9 us
    all_to_all x1, blocking collectives, local(): lax.all_to_all(column_block, 'ep', split_axis=0, concat_axis=0, tiled=True)  52.1 us
    all_to_all x1, waiting for transfers between devices, local(): lax.all_to_all(expert_rows, 'ep', split_axis=0, concat_axis=0, tiled=True)  35.8 us
    reduce_scatter x1, waiting for transfers between devices, local(): lax.psum_scatter(expert_partial.astype(jnp.bfloat16), 'tp', scatter_dimen...  23.5 us
    gather x2, local copies, waits for them, and re-layouts, local(): normalized[token_index]  19.9 us
    all_gather x2, blocking collectives, total_of_pieces(): parts = lax.all_gather(value, axis)  18.6 us
    all_to_all x1, starting transfers between devices, local(): lax.all_to_all(expert_rows, 'ep', split_axis=0, concat_axis=0, tiled=True)  11.1 us
    dot_general x1, matrix products, local(): jnp.dot(hidden, expert_down[0], preferred_element_type=jnp.float32)  10.3 us
  transfers between devices with their start and end apart: 5, of which 4 were waited for; matrix products, arithmetic and copies ran while one was open for 9% of the time, Pallas kernels for 0%

commit v1 on v0

--- a/solution.py
+++ b/solution.py
@@ -97,7 +97,9 @@
     first_column = lax.axis_index("tp") * quarter
     column_block = lax.dynamic_slice_in_dim(outgoing, first_column, quarter, 2)
     arrived = lax.all_to_all(column_block, "ep", split_axis=0, concat_axis=0, tiled=True)
-    arrived = lax.all_gather(arrived, "tp", axis=2, tiled=True)
+    arrived = jnp.concatenate(
+        lax.all_to_all(jnp.stack([arrived] * lax.axis_size("tp")), "tp", 0, 0), axis=2
+    )
     expert_input = arrived.reshape(experts * capacity, model_width)
     hidden = (
         jax.nn.silu(jnp.dot(expert_input, expert_gate[0], preferred_element_type=jnp.float32))

time: 313 us -> 299 us (0.955)
  waiting for transfers between devices: 125 us -> 54.5 us
  blocking collectives: 70.7 us -> 128 us
    all_gather x1 -> x0, waiting for transfers between devices: 64.9 us -> none  [local(): arrived = lax.all_gather(arrived, 'tp', axis=2, tiled=True)]
    all_to_all x0 -> x1, blocking collectives: none -> 56.6 us  [local(): lax.all_to_all(jnp.stack([arrived] * lax.axis_size('tp')), 'tp', 0, 0)]
    reduce_scatter x1, waiting for transfers between devices: 23.5 us -> 18 us  [local(): lax.psum_scatter(expert_partial.astype(jnp.bfloat16), 'tp', scatter_dimen...]
    unnamed x22 -> x27, local copies, waits for them, and re-layouts: 2.18 us -> 6.34 us
    reshape x1, local copies, waits for them, and re-layouts: 7.77 us -> 3.64 us  [local(): jnp.concatenate(lax.all_to_all(jnp.stack([arrived] * lax.axis_size('tp'))...]
  transfers between devices with their start and end apart: 5 -> 4, of which waited for: 4 -> 3; matrix products, arithmetic and copies ran while one was open for 9% -> 10% of each run, Pallas kernels for 0% -> 0%
where the time goes in v1:
time: 299 us; the launch traced here: 298 us
  blocking collectives  128 us (43%)
  waiting for transfers between devices  54.5 us (18%)
  local copies, waits for them, and re-layouts  46.9 us (16%)
  matrix products  21.5 us (7%)
  starting transfers between devices  16.4 us (5%)
  other arithmetic  16.4 us (5%)
  between operations  14.4 us (5%)
    all_to_all x1, blocking collectives, local(): lax.all_to_all(jnp.stack([arrived] * lax.axis_size('tp')), 'tp', 0, 0)  56.6 us
    all_to_all x1, blocking collectives, local(): lax.all_to_all(column_block, 'ep', split_axis=0, concat_axis=0, tiled=True)  52 us
    all_to_all x1, waiting for transfers between devices, local(): lax.all_to_all(expert_rows, 'ep', split_axis=0, concat_axis=0, tiled=True)  35.8 us
    gather x2, local copies, waits for them, and re-layouts, local(): normalized[token_index]  19.9 us
    all_gather x2, blocking collectives, total_of_pieces(): parts = lax.all_gather(value, axis)  19.2 us
    reduce_scatter x1, waiting for transfers between devices, local(): lax.psum_scatter(expert_partial.astype(jnp.bfloat16), 'tp', scatter_dimen...  18 us
    all_to_all x1, starting transfers between devices, local(): lax.all_to_all(expert_rows, 'ep', split_axis=0, concat_axis=0, tiled=True)  11.1 us
    dot_general x1, matrix products, local(): jnp.dot(hidden, expert_down[0], preferred_element_type=jnp.float32)  10.3 us
  transfers between devices with their start and end apart: 4, of which 3 were waited for; matrix products, arithmetic and copies ran while one was open for 10% of the time, Pallas kernels for 0%

profile of v1, /device:TPU:1, one launch (start us, length us, event | category | flops | bytes accessed | tf_op | source)
XLA Modules:
  0.0 297.8 jit_solution(13687065737893794231)
XLA Ops:
  7.2 0.0 copy-start
  7.2 0.0 reduce-scatter.5.cloned.1.call-start
  7.2 1.0 copy.31
  8.2 0.1 eq.29
  8.3 0.1 eq.25
  8.5 0.7 broadcast_multiply_fusion
  9.2 1.8 reduce-window.6
  11.0 0.3 slice_reduce_fusion
  11.3 0.1 copy.30
  11.4 0.2 mul.517
  11.6 0.1 fusion.60
  11.8 3.4 %scatter_custom_fusion = s32[1152]{0:T(1024)S(1)} fusion(s32[768]{0:T(1024)S(1)} %fusion.68, s32[768]{0:T(1024)S(1)} %iota.11, s32[]{:T(128)} %constant.26.clone.1), kind=kCustom, calls=%fused_computation.127 | custom fusion | bytes 4612 | tf_op jit(solution)/shard_map/scatter | solution.py:90
  15.2 0.0 copy-start.1
  15.2 0.0 copy-start.6
  15.2 1.8 convert_reduce_fusion
  17.1 0.0 copy-done.1
  17.1 0.6 fusion.2
  17.6 0.0 copy-done.6
  17.6 1.7 fusion.4
  19.3 12.3 %gather_fusion = bf16[1152,2048]{1,0:T(8,128)(2,1)} fusion(bf16[384,2048]{1,0:T(8,128)(2,1)} %fusion.4, s32[2048]{0:T(1024)S(1)} %pad_clamp_fusion), kind=kCustom, calls=%fused_computation | custom fusion | bytes 9441792 | tf_op jit(solution)/shard_map/gather | solution.py:94
  31.6 7.6 %gather.9 = bf16[64,18,2048]{2,1,0:T(8,128)(2,1)} reshape(bf16[1152,2048]{1,0:T(8,128)(2,1)} %gather_fusion) | data formatting | bytes 9437184 | tf_op jit(solution)/shard_map/gather | solution.py:94
  39.2 0.1 broadcast_in_dim.21
  39.3 1.8 dynamic-slice_select_fusion
  41.2 52.0 %all_to_all.15 = bf16[64,18,512]{2,1,0:T(8,128)(2,1)S(1)} all-to-all(bf16[64,18,512]{2,1,0:T(8,128)(2,1)S(1)} %dynamic-slice_select_fusion), channel_id=1, replica_groups=mesh['ep'=64,'tp'=4] {'ep'}, dimensions={0} | all-to-all | bytes 2359296 | tf_op jit(solution)/shard_map/all_to_all | solution.py:99
  93.2 0.4 copy.34
  93.5 0.6 stack.2
  94.1 56.6 %all_to_all.16 = bf16[4,64,18,512]{3,1,2,0:T(8,128)(2,1)S(1)} all-to-all(bf16[4,64,18,512]{3,1,2,0:T(8,128)(2,1)S(1)} %stack.2), channel_id=1, replica_groups=mesh['ep'=64,'tp'=4] {'tp'}, dimensions={0} | all-to-all | bytes 9437184 | tf_op jit(solution)/shard_map/all_to_all | solution.py:101
  150.7 3.6 %copy.35 = bf16[64,18,4,512]{3,2,1,0:T(4,128)(2,1)S(1)} copy(bf16[64,18,4,512]{3,0,1,2:T(8,128)(2,1)S(1)} %bitcast.73) | data formatting | bytes 9437184 | tf_op jit(solution)/shard_map/reshape | solution.py:100
  154.3 0.0 copy-start.8
  154.4 2.0 copy.37
  156.4 0.0 copy-start.2
  156.4 2.2 copy-done.2
  158.5 0.0 copy-done.8
  158.5 2.4 fusion.16
  160.9 10.3 %convolution_convert_fusion = bf16[1152,2048]{1,0:T(8,128)(2,1)} fusion(bf16[1152,2048]{1,0:T(8,128)(2,1)} %bitcast.76, f32[1152,256]{1,0:T(8,128)} %fusion.16, bf16[1,256,2048]{2,1,0:T(8,128)(2,1)} %param.26, bf16[1,2048,256]{2,1,0:T(8,128)(2,1)} %param.25), kind=kOutput, calls=%fused_computation.3 | convolution fusion | flops 2420047872 | bytes 12713984 | tf_op jit(solution)/shard_map/dot_general | solution.py:108
  171.2 0.0 reduce-scatter.5.cloned.1.call-update
  171.2 0.0 reduce-scatter.3.cloned.1.call-start
  171.3 0.9 copy-done.3
  172.2 0.1 copy-done.4
  172.3 0.2 multiply_convert_fusion.1
  172.6 5.3 %collective-permute-start = (bf16[30,512]{1,0:T(8,128)(2,1)S(1)}, bf16[30,512]{1,0:T(8,128)(2,1)S(1)}, u32[]{:S(2)}, u32[]{:S(2)}) collective-permute-start(bf16[30,512]{1,0:T(8,128)(2,1)S(1)} %slice.265), channel_id=1, source_target_pairs={{0,4},{4,8},{8,12},{12,16},{16,20},{20,24},{24,28},{28,32},{32,36}... | collective-permute-start | bytes 92168 | tf_op jit(solution)/shard_map/ppermute | solution.py:12
  177.8 0.0 copy-done.5
  177.9 0.7 collective-permute-done
  178.6 0.1 maximum_convert_fusion
  178.7 0.0 copy-start.10
  178.7 3.8 %fusion.72 = (f32[384]{0:T(512)S(1)}, f32[384]{0:T(512)S(1)}, f32[384,512]{1,0:T(8,128)S(1)}) fusion(f32[414,512]{1,0:T(8,128)S(1)} %maximum_convert_fusion, f32[512]{0:T(512)S(1)} %bitcast.108, f32[512]{0:T(512)S(1)} %bitcast.107, f32[512]{0:T(512)S(1)} %bitcast.106, f32[512]{0:T(512)S(1)} %bitcast.105, f32[512]{0:T(512)S(1)} %bitcast.104, ...), kind=kLoop, calls=%fused_computation.138 | loop fusion | flops 12582144 | bytes 25232384 | tf_op jit(solution)/shard_map/reduce_sum | solution.py:57
  182.6 9.6 %all-gather.2 = f32[4,1,384]{2,1,0:T(1,128)S(1)} all-gather(f32[1,1,384]{2,1,0:T(1,128)S(1)} %reshape.132), channel_id=2, replica_groups=mesh['ep'=64,'tp'=4] {'tp'}, dimensions={0}, use_global_device_ids=true | all-gather | bytes 7680 | tf_op jit(solution)/shard_map/all_gather | solution.py:16
  192.2 9.6 %all-gather.3 = f32[4,1,384]{2,1,0:T(1,128)S(1)} all-gather(f32[1,1,384]{2,1,0:T(1,128)S(1)} %reshape.134), channel_id=3, replica_groups=mesh['ep'=64,'tp'=4] {'tp'}, dimensions={0}, use_global_device_ids=true | all-gather | bytes 7680 | tf_op jit(solution)/shard_map/all_gather | solution.py:16
  201.8 0.0 copy-done
  201.8 0.0 copy-done.10
  201.9 2.3 convolution_convert_fusion.1
  204.2 0.0 reduce-scatter.3.cloned.1.call-update
  204.2 18.0 %reduce-scatter.5.cloned.1.call-done = bf16[1152,512]{1,0:T(8,128)(2,1)} async-done(((bf16[1152,2048]{1,0:T(8,128)(2,1)}), bf16[1152,512]{1,0:T(8,128)(2,1)}) %reduce-scatter.5.cloned.1.call-update) | async-done | bytes 1179664 | tf_op jit(solution)/shard_map/reduce_scatter | solution.py:113
  222.2 3.0 %reshape.102 = bf16[64,18,512]{2,1,0:T(8,128)(2,1)} reshape(bf16[1152,512]{1,0:T(8,128)(2,1)} %reduce-scatter.5.cloned.1.call-done) | data formatting | bytes 2359296 | tf_op jit(solution)/shard_map/reshape | solution.py:118
  225.2 11.1 %all-to-all-start.2 = ((bf16[64,18,512]{2,1,0:T(8,128)(2,1)}), bf16[64,18,512]{2,1,0:T(8,128)(2,1)}, u32[]{:S(2)}, u32[]{:S(2)}) async-start(bf16[64,18,512]{2,1,0:T(8,128)(2,1)} %reshape.102), calls=%async_computation.4 | async-start | bytes 3145728 | tf_op jit(solution)/shard_map/all_to_all | solution.py:119
  236.3 0.1 copy.29
  236.4 3.1 %fusion.76 = f32[384,256]{1,0:T(8,128)} fusion(bf16[384,2048]{1,0:T(8,128)(2,1)} %fusion.4, bf16[2048,256]{1,0:T(8,128)(2,1)} %param.27), kind=kOutput, calls=%fused_computation.141 | convolution fusion | flops 402653184 | bytes 3014656 | tf_op jit(solution)/shard_map/dot_general | solution.py:22
  239.5 35.8 %all-to-all-done.2 = bf16[64,18,512]{2,1,0:T(8,128)(2,1)} async-done(((bf16[64,18,512]{2,1,0:T(8,128)(2,1)}), bf16[64,18,512]{2,1,0:T(8,128)(2,1)}, u32[]{:S(2)}, u32[]{:S(2)}) %all-to-all-start.2) | async-done | bytes 1179680 | tf_op jit(solution)/shard_map/all_to_all | solution.py:119
  275.3 2.3 reshape.103
  277.6 3.3 %gather_fusion.1 = bf16[768,512]{1,0:T(8,128)(2,1)} fusion(bf16[1152,512]{1,0:T(8,128)(2,1)S(1)} %reshape.103, s32[1024]{0:T(1024)S(1)} %pad_clamp_fusion.1), kind=kCustom, calls=%fused_computation.1 | custom fusion | bytes 1575936 | tf_op jit(solution)/shard_map/gather | solution.py:120
  280.9 3.0 reshape.104
  283.9 3.6 %multiply_reduce_fusion = f32[384,512]{1,0:T(8,128)S(1)} fusion(f32[384,2,512]{2,1,0:T(2,128)} %reshape.104, f32[384,2]{1,0:T(8,128)S(1)} %copy.29), kind=kLoop, calls=%fused_computation.15 | loop fusion | flops 589824 | bytes 2362368 | tf_op jit(solution)/shard_map/reduce_sum | solution.py:122
  287.5 0.0 copy-done.9
  287.5 3.4 %fusion.6 = bf16[384,512]{1,0:T(8,128)(2,1)} fusion(f32[384,512]{1,0:T(8,128)S(1)} %multiply_reduce_fusion, bf16[256,512]{1,0:T(8,128)(2,1)S(1)} %copy-done.9, bf16[384,2048]{1,0:T(8,128)(2,1)} %fusion.4, bf16[2048,256]{1,0:T(8,128)(2,1)} %param.28, f32[384,256]{1,0:T(8,128)} %fusion.76), kind=kOutput, calls=%fused_computation.17 | convolution fusion | flops 504299520 | bytes 4456448 | tf_op jit(solution)/shard_map/dot_general | solution.py:75
  (25 shorter events, 0.2 us)
Async XLA Ops:
  7.2 194.7 %copy-start = (bf16[512,2048]{1,0:T(8,128)(2,1)S(1)}, bf16[512,2048]{1,0:T(8,128)(2,1)}, u32[]{:S(2)}) copy-start(bf16[512,2048]{1,0:T(8,128)(2,1)} %param.19) | copy-start | bytes 6291460
  7.2 215.0 %reduce-scatter.5.cloned.1.call-start = ((), (), s32[]{:S(2)}) async-start(), calls=%async_computation.6 | async-start | bytes 5898240 | tf_op jit(solution)/shard_map/reduce_scatter | solution.py:113
  15.2 1.9 copy-start.1
  15.2 2.4 copy-start.6
  154.3 4.2 %copy-start.8 = (bf16[1,2048,256]{2,1,0:T(8,128)(2,1)S(1)}, bf16[1,2048,256]{2,1,0:T(8,128)(2,1)}, u32[]{:S(2)}) copy-start(bf16[1,2048,256]{2,1,0:T(8,128)(2,1)} %param.24) | copy-start | bytes 3145732
  156.4 2.2 copy-start.2
  171.2 1.0 copy-start.3
  171.2 1.1 copy-start.4
  171.2 6.6 %copy-start.5 = (bf16[31,512]{1,0:T(8,128)(2,1)S(1)}, bf16[31,512]{1,0:T(8,128)(2,1)}, u32[]{:S(2)}) copy-start(bf16[31,512]{1,0:T(8,128)(2,1)} %param.17) | copy-start | bytes 95236
  171.2 119.7 %reduce-scatter.3.cloned.1.call-start = ((), (), s32[]{:S(2)}) async-start(), calls=%async_computation.5 | async-start | bytes 1966080 | tf_op jit(solution)/shard_map/reduce_scatter | solution.py:110
  172.6 6.0 %collective-permute-start = (bf16[30,512]{1,0:T(8,128)(2,1)S(1)}, bf16[30,512]{1,0:T(8,128)(2,1)S(1)}, u32[]{:S(2)}, u32[]{:S(2)}) collective-permute-start(bf16[30,512]{1,0:T(8,128)(2,1)S(1)} %slice.265), channel_id=1, source_target_pairs={{0,4},{4,8},{8,12},{12,16},{16,20},{20,24},{24,28},{28,32},{32,36}... | collective-permute-start | bytes 92168 | tf_op jit(solution)/shard_map/ppermute | solution.py:12
  178.7 23.1 %copy-start.10 = (f32[512]{0:T(512)S(1)}, f32[512]{0:T(512)}, u32[]{:S(2)}) copy-start(f32[512]{0:T(512)} %param.18) | copy-start | bytes 6148
  225.2 11.1 %copy-start.7 = (f32[384,2]{0,1:T(2,128)S(1)}, f32[384,2]{0,1:T(2,128)}, u32[]{:S(2)}) copy-start(f32[384,2]{0,1:T(2,128)} %param.23) | copy-start | bytes 9220
  225.2 50.1 %all-to-all-start.2 = ((bf16[64,18,512]{2,1,0:T(8,128)(2,1)}), bf16[64,18,512]{2,1,0:T(8,128)(2,1)}, u32[]{:S(2)}, u32[]{:S(2)}) async-start(bf16[64,18,512]{2,1,0:T(8,128)(2,1)} %reshape.102), calls=%async_computation.4 | async-start | bytes 3145728 | tf_op jit(solution)/shard_map/all_to_all | solution.py:119
  283.9 3.6 %copy-start.9 = (bf16[256,512]{1,0:T(8,128)(2,1)S(1)}, bf16[256,512]{1,0:T(8,128)(2,1)}, u32[]{:S(2)}) copy-start(bf16[256,512]{1,0:T(8,128)(2,1)} %param.29) | copy-start | bytes 786436
Sparse Core Ops, SparseCore 0:
  171.4 50.7 reduce-scatter.4
  225.3 26.9 reduce-scatter.2
